TPU v7x, 32 devices: a whole 2x2x4 slice. The times are simulated.
32 devices in a mesh: fs: 8 (over z, y), tp: 4 (over x, core).
Axes of the slice: x: 2, y: 2, z: 4, core: 2. Of those that a mesh axis runs over, the one named last changes fastest.
Arguments:
- tokens: bfloat16 [640, 3072], P('tp'), may hold values from -6 to 6
- gain_first: float32 [3072], replicated, may hold values from 0.1 to 1.9
- gain_second: float32 [3072], replicated, may hold values from 0.1 to 1.9
- gate_first: float32 [3072, 8192], P('fs', 'tp'), may hold values from -0.109375 to 0.109375
- up_first: float32 [3072, 8192], P('fs', 'tp'), may hold values from -0.109375 to 0.109375
- down_first: float32 [8192, 3072], P('fs', 'tp'), may hold values from -0.09375 to 0.09375
- gate_second: float32 [3072, 8192], P('fs', 'tp'), may hold values from -0.109375 to 0.109375
- up_second: float32 [3072, 8192], P('fs', 'tp'), may hold values from -0.109375 to 0.109375
- down_second: float32 [8192, 3072], P('fs', 'tp'), may hold values from -0.09375 to 0.09375
Outputs:
- result_rows: bfloat16 [640, 3072], P('tp')
- serve_gate_first: bfloat16 [3072, 8192], P(None, 'fs')
- serve_up_first: bfloat16 [3072, 8192], P(None, 'fs')
- serve_down_first: bfloat16 [8192, 3072], P('fs')
- serve_gate_second: bfloat16 [3072, 8192], P(None, 'fs')
- serve_up_second: bfloat16 [3072, 8192], P(None, 'fs')
- serve_down_second: bfloat16 [8192, 3072], P('fs')
All inputs are finite; a program needn't handle non-finite values.
Results may differ from a plain program's by a relative error of at most 0.011.
Values may be sent and summed in bfloat16 or wider, within the bound.
A program may use at most 192 MiB of HBM per device.

v0:
```python
import jax
import jax.numpy as jnp
from jax import lax
from jax.sharding import PartitionSpec as P


def plain_norm(values):
    values = values.astype(jnp.float32)
    center = jnp.mean(values, axis=-1, keepdims=True)
    spread = jnp.mean(jnp.square(values - center), axis=-1, keepdims=True)
    return (values - center) * lax.rsqrt(spread + 1e-05)


def sum_over_hidden(partial_value):
    pieces = lax.all_to_all(
        partial_value.astype(jnp.bfloat16), "fs", split_axis=1, concat_axis=0, tiled=True
    )
    rows = partial_value.shape[0]
    pieces = pieces.reshape(-1, rows, pieces.shape[1]).astype(jnp.float32)
    summed = jnp.sum(pieces, axis=0).astype(jnp.bfloat16)
    return lax.all_gather(summed, "fs", axis=1, tiled=True).astype(jnp.float32)


def regroup(folded):
    spread = lax.all_to_all(folded, "tp", split_axis=0, concat_axis=1, tiled=True)
    parts = lax.axis_size("fs")
    rows = spread.shape[0]
    owned = lax.all_to_all(spread, "fs", split_axis=1, concat_axis=0, tiled=True)
    owned = owned.reshape(parts, rows, owned.shape[1])
    whole = lax.all_gather(owned, "tp", axis=1, tiled=True)
    return whole.reshape(-1, whole.shape[2])


def half_step(normed, scales, w_gate, w_rising, w_down):
    gate_part = jnp.dot(normed, w_gate, preferred_element_type=jnp.float32)
    rising = jnp.dot(normed, w_rising, preferred_element_type=jnp.float32)
    hidden = (jax.nn.silu(gate_part) * rising).astype(jnp.bfloat16)
    partial_value = jnp.dot(hidden, w_down, preferred_element_type=jnp.float32)
    block = sum_over_hidden(partial_value)
    mixed = 1.6817928 * scales[None, :] * normed.astype(jnp.float32) + 0.5 * block
    return plain_norm(mixed).astype(jnp.bfloat16)


def on_device(
    tokens,
    gain_first,
    gain_second,
    gate_first,
    up_first,
    down_first,
    gate_second,
    up_second,
    down_second,
):
    row_count = gate_first.shape[0]
    offset = lax.axis_index("fs") * row_count

    def fold_gain(weight, scales):
        picked = lax.dynamic_slice_in_dim(scales, offset, row_count, 0)
        return (picked[:, None] * weight).astype(jnp.bfloat16)

    serve_gate_first = regroup(fold_gain(gate_first, gain_first))
    serve_up_first = regroup(fold_gain(up_first, gain_first))
    serve_down_first = lax.all_gather(down_first.astype(jnp.bfloat16), "tp", axis=1, tiled=True)
    serve_gate_second = regroup(fold_gain(gate_second, gain_second))
    serve_up_second = regroup(fold_gain(up_second, gain_second))
    serve_down_second = lax.all_gather(down_second.astype(jnp.bfloat16), "tp", axis=1, tiled=True)
    normed_zero = plain_norm(tokens).astype(jnp.bfloat16)
    normed_one = half_step(
        normed_zero, gain_first, serve_gate_first, serve_up_first, serve_down_first
    )
    result_rows = half_step(
        normed_one, gain_second, serve_gate_second, serve_up_second, serve_down_second
    )
    return (
        result_rows,
        serve_gate_first,
        serve_up_first,
        serve_down_first,
        serve_gate_second,
        serve_up_second,
        serve_down_second,
    )


def solution(mesh):
    placed = (
        P("tp", None),
        P(),
        P(),
        P("fs", "tp"),
        P("fs", "tp"),
        P("fs", "tp"),
        P("fs", "tp"),
        P("fs", "tp"),
        P("fs", "tp"),
    )
    return jax.shard_map(
        on_device,
        mesh=mesh,
        in_specs=placed,
        out_specs=(
            P("tp", None),
            P(None, "fs"),
            P(None, "fs"),
            P("fs", None),
            P(None, "fs"),
            P(None, "fs"),
            P("fs", None),
        ),
        check_vma=False,
    )
```

profile of v0, /device:TPU:0, one launch (start us, length us, event | category | flops | bytes accessed | tf_op | source)
XLA Modules:
  0.0 523.0 jit_solution(2696292961990616382)
XLA Ops:
  8.0 3.7 multiply_convert_fusion.3
  11.7 24.1 %all_to_all.154 = bf16[4,96,2048]{2,1,0:T(8,128)(2,1)S(1)} all-to-all(bf16[4,96,2048]{2,1,0:T(8,128)(2,1)S(1)} %bitcast.44), channel_id=1, replica_groups=mesh['fs'=8,'tp'=4] {'tp'}, dimensions={0} | all-to-all | bytes 3145728 | tf_op jit(solution)/shard_map/all_to_all | solution.py:25
  35.8 1.2 copy.28
  37.0 1.8 all_to_all.119
  38.9 2.3 copy.29
  41.2 42.3 %all_to_all.155 = bf16[96,8,1024]{2,0,1:T(8,128)(2,1)S(1)} all-to-all(bf16[96,8,1024]{2,0,1:T(8,128)(2,1)S(1)} %copy.29), channel_id=1, replica_groups=mesh['fs'=8,'tp'=4] {'fs'}, dimensions={1} | all-to-all | bytes 3145728 | tf_op jit(solution)/shard_map/all_to_all | solution.py:28
  83.5 2.0 copy.30
  85.6 36.1 %all_to_all.156 = bf16[4,96,2048]{2,1,0:T(8,128)(2,1)S(1)} all-to-all(bf16[4,96,2048]{2,1,0:T(8,128)(2,1)S(1)} %bitcast.42), channel_id=1, replica_groups=mesh['fs'=8,'tp'=4] {'tp'}, dimensions={0} | all-to-all | bytes 3145728 | tf_op jit(solution)/shard_map/all_to_all | solution.py:25
  121.7 1.2 copy.32
  123.3 0.9 copy.33
  124.2 39.1 %all_to_all.157 = bf16[96,8,1024]{2,0,1:T(8,128)(2,1)S(1)} all-to-all(bf16[96,8,1024]{2,0,1:T(8,128)(2,1)S(1)} %copy.33), channel_id=1, replica_groups=mesh['fs'=8,'tp'=4] {'fs'}, dimensions={1} | all-to-all | bytes 3145728 | tf_op jit(solution)/shard_map/all_to_all | solution.py:28
  163.3 2.0 copy.34
  165.4 1.3 convert_element_type.64
  166.8 3.9 multiply_convert_fusion.1
  170.7 39.8 %all_to_all.158 = bf16[4,96,2048]{2,1,0:T(8,128)(2,1)S(1)} all-to-all(bf16[4,96,2048]{2,1,0:T(8,128)(2,1)S(1)} %bitcast.45), channel_id=1, replica_groups=mesh['fs'=8,'tp'=4] {'tp'}, dimensions={0} | all-to-all | bytes 3145728 | tf_op jit(solution)/shard_map/all_to_all | solution.py:25
  210.5 1.2 copy.37
  211.7 1.8 all_to_all.133
  213.6 2.3 copy.38
  215.8 51.1 %all_to_all.159 = bf16[96,8,1024]{2,0,1:T(8,128)(2,1)S(1)} all-to-all(bf16[96,8,1024]{2,0,1:T(8,128)(2,1)S(1)} %copy.38), channel_id=1, replica_groups=mesh['fs'=8,'tp'=4] {'fs'}, dimensions={1} | all-to-all | bytes 3145728 | tf_op jit(solution)/shard_map/all_to_all | solution.py:28
  266.9 2.0 copy.39
  269.0 26.1 %all_to_all.160 = bf16[4,96,2048]{2,1,0:T(8,128)(2,1)S(1)} all-to-all(bf16[4,96,2048]{2,1,0:T(8,128)(2,1)S(1)} %bitcast.43), channel_id=1, replica_groups=mesh['fs'=8,'tp'=4] {'tp'}, dimensions={0} | all-to-all | bytes 3145728 | tf_op jit(solution)/shard_map/all_to_all | solution.py:25
  295.1 1.2 copy.41
  296.8 0.9 copy.42
  297.6 39.2 %all_to_all.161 = bf16[96,8,1024]{2,0,1:T(8,128)(2,1)S(1)} all-to-all(bf16[96,8,1024]{2,0,1:T(8,128)(2,1)S(1)} %copy.42), channel_id=1, replica_groups=mesh['fs'=8,'tp'=4] {'fs'}, dimensions={1} | all-to-all | bytes 3145728 | tf_op jit(solution)/shard_map/all_to_all | solution.py:28
  336.8 2.0 copy.43
  338.9 1.3 convert_element_type.72
  340.2 1.2 copy-done.1
  342.0 9.7 %copy.31 = bf16[8,384,1024]{2,1,0:T(8,128)(2,1)} copy(bf16[8,384,1024]{2,0,1:T(8,128)(2,1)} %all-gather.7.cloned.1.call-done) | data formatting | bytes 12582912 | tf_op jit(solution)/shard_map/all_gather | solution.py:30
  351.7 9.2 %copy.35 = bf16[8,384,1024]{2,1,0:T(8,128)(2,1)} copy(bf16[8,384,1024]{2,0,1:T(8,128)(2,1)} %all-gather.9.cloned.1.call-done) | data formatting | bytes 12582912 | tf_op jit(solution)/shard_map/all_gather | solution.py:30
  360.9 1.3 fusion.14
  362.3 7.0 %convolution_convert_fusion.1 = bf16[160,3072]{1,0:T(8,128)(2,1)S(1)} fusion(bf16[1024,3072]{1,0:T(8,128)(2,1)} %all-gather.11.cloned.1.call-done, bf16[3072,1024]{1,0:T(8,128)(2,1)} %bitcast.38, f32[160,1024]{1,0:T(8,128)S(1)} %fusion.14, bf16[160,3072]{1,0:T(8,128)(2,1)S(1)} %copy-done.1, f32[160]{0:T(256)S(1)} %add_rsqrt_fusion.2, ...), kind=kOutput, calls=%fused_computation.1 | convolution fusion | flops 2016706560 | bytes 15205632 | tf_op jit(solution)/shard_map/dot_general | solution.py:38
  369.3 1.0 copy.51
  370.3 3.8 all-to-all-start.4
  374.1 9.1 %copy.40 = bf16[8,384,1024]{2,1,0:T(8,128)(2,1)} copy(bf16[8,384,1024]{2,0,1:T(8,128)(2,1)} %all-gather.13.cloned.1.call-done) | data formatting | bytes 12582912 | tf_op jit(solution)/shard_map/all_gather | solution.py:30
  383.7 9.0 %copy.44 = bf16[8,384,1024]{2,1,0:T(8,128)(2,1)} copy(bf16[8,384,1024]{2,0,1:T(8,128)(2,1)} %all-gather.15.cloned.1.call-done) | data formatting | bytes 12582912 | tf_op jit(solution)/shard_map/all_gather | solution.py:30
  392.7 5.5 %all-to-all-done.4 = bf16[160,8,384]{2,0,1:T(8,128)(2,1)S(1)} async-done(((bf16[160,8,384]{2,0,1:T(8,128)(2,1)}), bf16[160,8,384]{2,0,1:T(8,128)(2,1)S(1)}, u32[]{:S(2)}, u32[]{:S(2)}) %all-to-all-start.4) | async-done | bytes 983072 | tf_op jit(solution)/shard_map/all_to_all | solution.py:15
  398.3 33.7 %all_gather.27 = bf16[160,3072]{1,0:T(8,128)(2,1)S(1)} all-gather(bf16[160,384]{1,0:T(8,128)(2,1)S(1)} %reduce_sum.80), channel_id=1, replica_groups=mesh['fs'=8,'tp'=4] {'fs'}, dimensions={1}, use_global_device_ids=true | all-gather | bytes 1105920 | tf_op jit(solution)/shard_map/all_gather | solution.py:21
  432.6 0.8 multiply_reduce_fusion.1
  433.4 0.9 multiply_convert_fusion.5
  434.7 1.3 fusion.16
  436.0 6.9 %convolution_convert_fusion = bf16[160,3072]{1,0:T(8,128)(2,1)S(1)} fusion(bf16[1024,3072]{1,0:T(8,128)(2,1)} %all-gather.17.cloned.1.call-done, bf16[160,3072]{1,0:T(8,128)(2,1)S(1)} %multiply_convert_fusion.5, bf16[3072,1024]{1,0:T(8,128)(2,1)} %bitcast.40, f32[160,1024]{1,0:T(8,128)S(1)} %fusion.16), kind=kOutput, calls=%fused_computation | convolution fusion | flops 2014740480 | bytes 15204352 | tf_op jit(solution)/shard_map/dot_general | solution.py:38
  442.9 1.0 copy.50
  444.0 3.6 all-to-all-start.9
  447.6 23.0 %all-to-all-done.9 = bf16[160,8,384]{2,0,1:T(8,128)(2,1)S(1)} async-done(((bf16[160,8,384]{2,0,1:T(8,128)(2,1)}), bf16[160,8,384]{2,0,1:T(8,128)(2,1)S(1)}, u32[]{:S(2)}, u32[]{:S(2)}) %all-to-all-start.9) | async-done | bytes 983072 | tf_op jit(solution)/shard_map/all_to_all | solution.py:15
  470.6 33.6 %all_gather.31 = bf16[160,3072]{1,0:T(8,128)(2,1)S(1)} all-gather(bf16[160,384]{1,0:T(8,128)(2,1)S(1)} %reduce_sum.83), channel_id=1, replica_groups=mesh['fs'=8,'tp'=4] {'fs'}, dimensions={1}, use_global_device_ids=true | all-gather | bytes 1105920 | tf_op jit(solution)/shard_map/all_gather | solution.py:21
  505.4 1.5 multiply_convert_fusion.4
  506.9 6.1 %copy.54 = bf16[1024,3072]{1,0:T(8,128)(2,1)} copy(bf16[1024,3072]{1,0:T(8,128)(2,1)} %all-gather.11.cloned.1.call-done) | data formatting | bytes 12582912
  513.0 2.7 copy.55
  (55 shorter events, 5.7 us)
Async XLA Ops:
  7.2 334.9 %all-gather.7.cloned.1.call-start = ((), (), s32[]{:S(2)}) async-start(), calls=%async_computation.10 | async-start | bytes 7864320 | tf_op jit(solution)/shard_map/all_gather | solution.py:30
  85.5 266.2 %all-gather.9.cloned.1.call-start = ((), (), s32[]{:S(2)}) async-start(), calls=%async_computation.11 | async-start | bytes 7864320 | tf_op jit(solution)/shard_map/all_gather | solution.py:30
  163.3 2.1 copy-start.3
  165.3 1.4 copy-start.6
  165.3 196.9 %all-gather.11.cloned.1.call-start = ((), (), s32[]{:S(2)}) async-start(), calls=%async_computation.12 | async-start | bytes 7864320 | tf_op jit(solution)/shard_map/all_gather | solution.py:64
  166.7 207.4 %all-gather.13.cloned.1.call-start = ((), (), s32[]{:S(2)}) async-start(), calls=%async_computation.13 | async-start | bytes 7864320 | tf_op jit(solution)/shard_map/all_gather | solution.py:30
  269.0 114.7 %all-gather.15.cloned.1.call-start = ((), (), s32[]{:S(2)}) async-start(), calls=%async_computation.14 | async-start | bytes 7864320 | tf_op jit(solution)/shard_map/all_gather | solution.py:30
  336.8 2.1 copy-start.4
  338.8 97.2 %all-gather.17.cloned.1.call-start = ((), (), s32[]{:S(2)}) async-start(), calls=%async_computation.15 | async-start | bytes 7864320 | tf_op jit(solution)/shard_map/all_gather | solution.py:67
  340.2 1.2 copy-start.1
  351.7 9.2 %copy-start.2 = (bf16[8,384,1024]{2,1,0:T(8,128)(2,1)S(1)}, bf16[8,384,1024]{2,1,0:T(8,128)(2,1)}, u32[]{:S(2)}) copy-start(bf16[8,384,1024]{2,1,0:T(8,128)(2,1)} %copy.31) | copy-start | bytes 18874372
  369.3 4.8 copy-start.5
  370.3 27.8 %all-to-all-start.4 = ((bf16[160,8,384]{2,0,1:T(8,128)(2,1)}), bf16[160,8,384]{2,0,1:T(8,128)(2,1)S(1)}, u32[]{:S(2)}, u32[]{:S(2)}) async-start(bf16[160,8,384]{2,0,1:T(8,128)(2,1)} %bitcast.31), calls=%async_computation.4 | async-start | bytes 1966080 | tf_op jit(solution)/shard_map/all_to_all | solution.py:15
  432.0 2.8 copy-start
  444.0 26.5 %all-to-all-start.9 = ((bf16[160,8,384]{2,0,1:T(8,128)(2,1)}), bf16[160,8,384]{2,0,1:T(8,128)(2,1)S(1)}, u32[]{:S(2)}, u32[]{:S(2)}) async-start(bf16[160,8,384]{2,0,1:T(8,128)(2,1)} %bitcast.30), calls=%async_computation.9 | async-start | bytes 1966080 | tf_op jit(solution)/shard_map/all_to_all | solution.py:15
  505.4 7.6 %slice-start = ((s8[6291456]{0:T(1024)(128)(4,1)}), s8[4194304]{0:T(1024)(128)(4,1)S(1)}, s32[]{:S(2)}) async-start(s8[6291456]{0:T(1024)(128)(4,1)} %bitcast.34), calls=%async_computation.16 | async-start | bytes 8388608
  506.9 6.1 %slice-start.1 = ((s8[6291456]{0:T(1024)(128)(4,1)}), s8[2097152]{0:T(1024)(128)(4,1)S(1)}, s32[]{:S(2)}) async-start(s8[6291456]{0:T(1024)(128)(4,1)} %bitcast.34), calls=%async_computation.17 | async-start | bytes 4194304
Sparse Core Ops, SparseCore 0:
  85.6 57.7 all-gather.6
  165.4 61.2 all-gather.8
  228.8 46.1 all-gather.10
  276.5 50.4 all-gather.12
  338.9 44.6 all-gather.14
  385.7 46.3 all-gather.16
where the time goes:
time: 532 us; the launch traced here: 523 us
  blocking collectives  365 us (69%)
  local copies, waits for them, and re-layouts  74 us (14%)
  waiting for transfers between devices  29.1 us (5%)
  matrix products  16.4 us (3%)
  other arithmetic  16.1 us (3%)
  between operations  14.8 us (3%)
  starting transfers between devices  7.57 us (1%)
    all_to_all x4, blocking collectives, regroup(): lax.all_to_all(spread, 'fs', split_axis=1, concat_axis=0, tiled=True)  172 us
    all_to_all x4, blocking collectives, regroup(): lax.all_to_all(folded, 'tp', split_axis=0, concat_axis=1, tiled=True)  126 us
    all_gather x2, blocking collectives, sum_over_hidden(): return lax.all_gather(summed, 'fs', axis=1, tiled=True).astype(jnp.float32)  67.3 us
    all_gather x4, local copies, waits for them, and re-layouts, regroup(): whole = lax.all_gather(owned, 'tp', axis=1, tiled=True)  36.9 us
    all_to_all x2, waiting for transfers between devices, sum_over_hidden(): lax.all_to_all(partial_value.astype(jnp.bfloat16), 'fs', split_axis=1, co...  28.4 us
    all_to_all x12, local copies, waits for them, and re-layouts, regroup(): lax.all_to_all(spread, 'fs', split_axis=1, concat_axis=0, tiled=True)  18.8 us
    dot_general x2, matrix products, half_step(): partial_value = jnp.dot(hidden, w_down, preferred_element_type=jnp.float32)  13.9 us
  transfers between devices with their start and end apart: 8, of which 3 were waited for; matrix products, arithmetic and copies ran while one was open for 14% of the time, Pallas kernels for 0%

commit v1 on v0

--- a/solution.py
+++ b/solution.py
@@ -2,6 +2,13 @@
 import jax.numpy as jnp
 from jax import lax
 from jax.sharding import PartitionSpec as P
+
+
+def swapped_in(x, name, d):
+    devices = lax.axis_size(name)
+    tiles = jnp.stack([x for _ in range(devices)])
+    tiles = lax.all_to_all(tiles, name, split_axis=0, concat_axis=0)
+    return jnp.concatenate(tiles, axis=d)
 
 
 def plain_norm(values):
@@ -18,7 +25,7 @@
     rows = partial_value.shape[0]
     pieces = pieces.reshape(-1, rows, pieces.shape[1]).astype(jnp.float32)
     summed = jnp.sum(pieces, axis=0).astype(jnp.bfloat16)
-    return lax.all_gather(summed, "fs", axis=1, tiled=True).astype(jnp.float32)
+    return swapped_in(summed, "fs", 1).astype(jnp.float32)
 
 
 def regroup(folded):

time: 532 us -> 526 us (0.989)
  blocking collectives: 365 us -> 355 us
    all_gather x2 -> x0, blocking collectives: 67.3 us -> none  [sum_over_hidden(): return lax.all_gather(summed, 'fs', axis=1, tiled=True).astype(jnp.float32)]
    all_to_all x0 -> x2, blocking collectives: none -> 57.3 us  [sum_over_hidden(): lax.all_to_all(partial_value.astype(jnp.bfloat16), 'fs', split_axis=1, co...]
where the time goes in v1:
time: 526 us; the launch traced here: 516 us
  blocking collectives  355 us (67%)
  local copies, waits for them, and re-layouts  73.8 us (14%)
  waiting for transfers between devices  32.3 us (6%)
  matrix products  16.8 us (3%)
  other arithmetic  15.7 us (3%)
  between operations  14.9 us (3%)
  starting transfers between devices  7.54 us (1%)
    all_to_all x4, blocking collectives, regroup(): lax.all_to_all(spread, 'fs', split_axis=1, concat_axis=0, tiled=True)  172 us
    all_to_all x4, blocking collectives, regroup(): lax.all_to_all(folded, 'tp', split_axis=0, concat_axis=1, tiled=True)  126 us
    all_to_all x2, blocking collectives, sum_over_hidden(): lax.all_to_all(partial_value.astype(jnp.bfloat16), 'fs', split_axis=1, co...  57.3 us
    all_gather x4, local copies, waits for them, and re-layouts, regroup(): whole = lax.all_gather(owned, 'tp', axis=1, tiled=True)  36.9 us
    all_to_all x2, waiting for transfers between devices, swapped_in(): tiles = lax.all_to_all(tiles, name, split_axis=0, concat_axis=0)  30.1 us
    all_to_all x12, local copies, waits for them, and re-layouts, regroup(): lax.all_to_all(spread, 'fs', split_axis=1, concat_axis=0, tiled=True)  18.8 us
    dot_general x2, matrix products, half_step(): partial_value = jnp.dot(hidden, w_down, preferred_element_type=jnp.float32)  14.2 us
  transfers between devices with their start and end apart: 8, of which 3 were waited for; matrix products, arithmetic and copies ran while one was open for 14% of the time, Pallas kernels for 0%

profile of v1, /device:TPU:0, one launch (start us, length us, event | category | flops | bytes accessed | tf_op | source)
XLA Modules:
  0.0 516.4 jit_solution(6241368712151512550)
XLA Ops:
  8.0 3.7 multiply_convert_fusion.3
  11.7 24.1 %all_to_all.164 = bf16[4,96,2048]{2,1,0:T(8,128)(2,1)S(1)} all-to-all(bf16[4,96,2048]{2,1,0:T(8,128)(2,1)S(1)} %bitcast.62), channel_id=1, replica_groups=mesh['fs'=8,'tp'=4] {'tp'}, dimensions={0} | all-to-all | bytes 3145728 | tf_op jit(solution)/shard_map/all_to_all | solution.py:32
  35.8 1.2 copy.46
  37.0 1.8 all_to_all.125
  38.9 2.3 copy.47
  41.2 42.3 %all_to_all.165 = bf16[96,8,1024]{2,0,1:T(8,128)(2,1)S(1)} all-to-all(bf16[96,8,1024]{2,0,1:T(8,128)(2,1)S(1)} %copy.47), channel_id=1, replica_groups=mesh['fs'=8,'tp'=4] {'fs'}, dimensions={1} | all-to-all | bytes 3145728 | tf_op jit(solution)/shard_map/all_to_all | solution.py:35
  83.5 2.0 copy.48
  85.6 36.1 %all_to_all.166 = bf16[4,96,2048]{2,1,0:T(8,128)(2,1)S(1)} all-to-all(bf16[4,96,2048]{2,1,0:T(8,128)(2,1)S(1)} %bitcast.60), channel_id=1, replica_groups=mesh['fs'=8,'tp'=4] {'tp'}, dimensions={0} | all-to-all | bytes 3145728 | tf_op jit(solution)/shard_map/all_to_all | solution.py:32
  121.7 1.2 copy.50
  123.3 0.9 copy.51
  124.2 39.1 %all_to_all.167 = bf16[96,8,1024]{2,0,1:T(8,128)(2,1)S(1)} all-to-all(bf16[96,8,1024]{2,0,1:T(8,128)(2,1)S(1)} %copy.51), channel_id=1, replica_groups=mesh['fs'=8,'tp'=4] {'fs'}, dimensions={1} | all-to-all | bytes 3145728 | tf_op jit(solution)/shard_map/all_to_all | solution.py:35
  163.3 2.0 copy.52
  165.4 1.3 convert_element_type.68
  166.8 3.9 multiply_convert_fusion.1
  170.7 39.8 %all_to_all.168 = bf16[4,96,2048]{2,1,0:T(8,128)(2,1)S(1)} all-to-all(bf16[4,96,2048]{2,1,0:T(8,128)(2,1)S(1)} %bitcast.63), channel_id=1, replica_groups=mesh['fs'=8,'tp'=4] {'tp'}, dimensions={0} | all-to-all | bytes 3145728 | tf_op jit(solution)/shard_map/all_to_all | solution.py:32
  210.5 1.2 copy.56
  211.7 1.8 all_to_all.140
  213.6 2.3 copy.57
  215.8 51.2 %all_to_all.169 = bf16[96,8,1024]{2,0,1:T(8,128)(2,1)S(1)} all-to-all(bf16[96,8,1024]{2,0,1:T(8,128)(2,1)S(1)} %copy.57), channel_id=1, replica_groups=mesh['fs'=8,'tp'=4] {'fs'}, dimensions={1} | all-to-all | bytes 3145728 | tf_op jit(solution)/shard_map/all_to_all | solution.py:35
  267.1 2.0 copy.58
  269.2 26.4 %all_to_all.170 = bf16[4,96,2048]{2,1,0:T(8,128)(2,1)S(1)} all-to-all(bf16[4,96,2048]{2,1,0:T(8,128)(2,1)S(1)} %bitcast.61), channel_id=1, replica_groups=mesh['fs'=8,'tp'=4] {'tp'}, dimensions={0} | all-to-all | bytes 3145728 | tf_op jit(solution)/shard_map/all_to_all | solution.py:32
  295.6 1.2 copy.60
  297.2 0.9 copy.61
  298.1 39.1 %all_to_all.171 = bf16[96,8,1024]{2,0,1:T(8,128)(2,1)S(1)} all-to-all(bf16[96,8,1024]{2,0,1:T(8,128)(2,1)S(1)} %copy.61), channel_id=1, replica_groups=mesh['fs'=8,'tp'=4] {'fs'}, dimensions={1} | all-to-all | bytes 3145728 | tf_op jit(solution)/shard_map/all_to_all | solution.py:35
  337.2 2.0 copy.62
  339.3 1.3 convert_element_type.76
  340.6 1.2 copy-done
  342.4 9.7 %copy.49 = bf16[8,384,1024]{2,1,0:T(8,128)(2,1)} copy(bf16[8,384,1024]{2,0,1:T(8,128)(2,1)} %all-gather.7.cloned.1.call-done) | data formatting | bytes 12582912 | tf_op jit(solution)/shard_map/all_gather | solution.py:37
  352.2 9.2 %copy.53 = bf16[8,384,1024]{2,1,0:T(8,128)(2,1)} copy(bf16[8,384,1024]{2,0,1:T(8,128)(2,1)} %all-gather.9.cloned.1.call-done) | data formatting | bytes 12582912 | tf_op jit(solution)/shard_map/all_gather | solution.py:37
  361.4 1.3 fusion.14
  362.7 7.1 %convolution_convert_fusion.1 = bf16[160,3072]{1,0:T(8,128)(2,1)S(1)} fusion(bf16[1024,3072]{1,0:T(8,128)(2,1)} %all-gather.11.cloned.1.call-done, bf16[3072,1024]{1,0:T(8,128)(2,1)} %bitcast.56, f32[160,1024]{1,0:T(8,128)S(1)} %fusion.14, bf16[160,3072]{1,0:T(8,128)(2,1)S(1)} %copy-done, f32[160]{0:T(256)S(1)} %add_rsqrt_fusion.2, ...), kind=kOutput, calls=%fused_computation.1 | convolution fusion | flops 2016706560 | bytes 15205632 | tf_op jit(solution)/shard_map/dot_general | solution.py:45
  369.9 27.1 %all_to_all.172 = bf16[160,8,384]{2,0,1:T(8,128)(2,1)S(1)} all-to-all(bf16[160,8,384]{2,0,1:T(8,128)(2,1)S(1)} %bitcast.72), channel_id=1, replica_groups=mesh['fs'=8,'tp'=4] {'fs'}, dimensions={1} | all-to-all | bytes 1966080 | tf_op jit(solution)/shard_map/all_to_all | solution.py:22
  397.2 1.0 stack.4
  398.2 3.7 all-to-all-start.5
  402.0 9.0 %copy.59 = bf16[8,384,1024]{2,1,0:T(8,128)(2,1)} copy(bf16[8,384,1024]{2,0,1:T(8,128)(2,1)} %all-gather.13.cloned.1.call-done) | data formatting | bytes 12582912 | tf_op jit(solution)/shard_map/all_gather | solution.py:37
  411.0 9.0 %copy.63 = bf16[8,384,1024]{2,1,0:T(8,128)(2,1)} copy(bf16[8,384,1024]{2,0,1:T(8,128)(2,1)} %all-gather.15.cloned.1.call-done) | data formatting | bytes 12582912 | tf_op jit(solution)/shard_map/all_gather | solution.py:37
  420.0 5.9 %all-to-all-done.5 = bf16[8,160,384]{2,1,0:T(8,128)(2,1)S(1)} async-done(((bf16[8,160,384]{2,1,0:T(8,128)(2,1)}), bf16[8,160,384]{2,1,0:T(8,128)(2,1)S(1)}, u32[]{:S(2)}, u32[]{:S(2)}) %all-to-all-start.5) | async-done | bytes 983072 | tf_op jit(solution)/shard_map/all_to_all | solution.py:10
  428.9 1.3 fusion.16
  430.2 2.0 all-gather.17.cloned.1.call-done
  432.2 7.2 %convolution_convert_fusion = bf16[160,3072]{1,0:T(8,128)(2,1)S(1)} fusion(bf16[1024,3072]{1,0:T(8,128)(2,1)} %all-gather.17.cloned.1.call-done, bf16[160,3072]{1,0:T(8,128)(2,1)S(1)} %multiply_convert_fusion.5, bf16[3072,1024]{1,0:T(8,128)(2,1)} %bitcast.58, f32[160,1024]{1,0:T(8,128)S(1)} %fusion.16), kind=kOutput, calls=%fused_computation | convolution fusion | flops 2014740480 | bytes 15204352 | tf_op jit(solution)/shard_map/dot_general | solution.py:45
  439.5 30.2 %all_to_all.173 = bf16[160,8,384]{2,0,1:T(8,128)(2,1)S(1)} all-to-all(bf16[160,8,384]{2,0,1:T(8,128)(2,1)S(1)} %bitcast.73), channel_id=1, replica_groups=mesh['fs'=8,'tp'=4] {'fs'}, dimensions={1} | all-to-all | bytes 1966080 | tf_op jit(solution)/shard_map/all_to_all | solution.py:22
  469.8 1.0 stack.5
  470.8 3.6 all-to-all-start.11
  474.4 24.2 %all-to-all-done.11 = bf16[8,160,384]{2,1,0:T(8,128)(2,1)S(1)} async-done(((bf16[8,160,384]{2,1,0:T(8,128)(2,1)}), bf16[8,160,384]{2,1,0:T(8,128)(2,1)S(1)}, u32[]{:S(2)}, u32[]{:S(2)}) %all-to-all-start.11) | async-done | bytes 983072 | tf_op jit(solution)/shard_map/all_to_all | solution.py:10
  499.9 1.4 multiply_convert_fusion.4
  501.8 3.2 copy.76
  505.0 1.4 slice-done.5
  506.4 2.7 copy.77
  (69 shorter events, 8.0 us)
Async XLA Ops:
  7.2 335.3 %all-gather.7.cloned.1.call-start = ((), (), s32[]{:S(2)}) async-start(), calls=%async_computation.12 | async-start | bytes 7864320 | tf_op jit(solution)/shard_map/all_gather | solution.py:37
  85.5 266.7 %all-gather.9.cloned.1.call-start = ((), (), s32[]{:S(2)}) async-start(), calls=%async_computation.13 | async-start | bytes 7864320 | tf_op jit(solution)/shard_map/all_gather | solution.py:37
  163.3 2.1 copy-start.2
  165.3 1.4 copy-start.5
  165.3 197.4 %all-gather.11.cloned.1.call-start = ((), (), s32[]{:S(2)}) async-start(), calls=%async_computation.14 | async-start | bytes 7864320 | tf_op jit(solution)/shard_map/all_gather | solution.py:71
  166.7 235.3 %all-gather.13.cloned.1.call-start = ((), (), s32[]{:S(2)}) async-start(), calls=%async_computation.15 | async-start | bytes 7864320 | tf_op jit(solution)/shard_map/all_gather | solution.py:37
  269.1 141.9 %all-gather.15.cloned.1.call-start = ((), (), s32[]{:S(2)}) async-start(), calls=%async_computation.16 | async-start | bytes 7864320 | tf_op jit(solution)/shard_map/all_gather | solution.py:37
  337.2 2.1 copy-start.3
  339.2 93.0 %all-gather.17.cloned.1.call-start = ((), (), s32[]{:S(2)}) async-start(), calls=%async_computation.17 | async-start | bytes 7864320 | tf_op jit(solution)/shard_map/all_gather | solution.py:74
  340.6 1.2 copy-start
  352.2 9.2 %copy-start.1 = (bf16[8,384,1024]{2,1,0:T(8,128)(2,1)S(1)}, bf16[8,384,1024]{2,1,0:T(8,128)(2,1)}, u32[]{:S(2)}) copy-start(bf16[8,384,1024]{2,1,0:T(8,128)(2,1)} %copy.49) | copy-start | bytes 18874372
  397.0 4.9 copy-start.4
  398.2 27.7 %all-to-all-start.5 = ((bf16[8,160,384]{2,1,0:T(8,128)(2,1)}), bf16[8,160,384]{2,1,0:T(8,128)(2,1)S(1)}, u32[]{:S(2)}, u32[]{:S(2)}) async-start(bf16[8,160,384]{2,1,0:T(8,128)(2,1)} %stack.4), calls=%async_computation.5 | async-start | bytes 1966080 | tf_op jit(solution)/shard_map/all_to_all | solution.py:10
  425.9 2.4 slice-start
  426.3 2.7 slice-start.1
  470.8 27.8 %all-to-all-start.11 = ((bf16[8,160,384]{2,1,0:T(8,128)(2,1)}), bf16[8,160,384]{2,1,0:T(8,128)(2,1)S(1)}, u32[]{:S(2)}, u32[]{:S(2)}) async-start(bf16[8,160,384]{2,1,0:T(8,128)(2,1)} %stack.5), calls=%async_computation.11 | async-start | bytes 1966080 | tf_op jit(solution)/shard_map/all_to_all | solution.py:10
  498.6 2.7 slice-start.2
  498.9 2.8 slice-start.3
  499.9 5.1 slice-start.4
  501.8 4.6 slice-start.5
Sparse Core Ops, SparseCore 0:
  85.6 57.7 all-gather.6
  165.4 61.2 all-gather.8
  228.8 46.1 all-gather.10
  276.5 50.5 all-gather.12
  339.3 44.4 all-gather.14
  385.8 46.3 all-gather.16
